TPU v7x, 512 devices: a whole 4x8x8 slice. The times are simulated.
512 devices in a mesh: ep: 32 (over z, x), tp: 16 (over y, core).
Axes of the slice: x: 4, y: 8, z: 8, core: 2. Of those that a mesh axis runs over, the one named last changes fastest.
Arguments:
- mixer_query: bfloat16 [8192, 2048], P('ep', 'tp'), may hold values from -6 to 6
- mixer_forget: bfloat16 [8192, 2048], P('ep', 'tp'), may hold values from -5.5 to 5.5
- mixer_value: bfloat16 [8192, 2048], P('ep', 'tp'), may hold values from -6 to 6
- mixer_gate: bfloat16 [8192, 2048], P('ep', 'tp'), may hold values from -6 to 6
- forget_floor: float32 [2048], P('tp'), may hold values from 0.88 to 1
- head_gain: float32 [128], replicated, may hold values from 0.1 to 1.9
- mixer_proj: bfloat16 [2048, 2048], P(None, 'tp'), may hold values from -0.125 to 0.125
- expert_tokens: bfloat16 [4096, 2048], P('ep'), may hold values from -6 to 6
- expert_gain: float32 [2048], replicated, may hold values from 0.1 to 1.9
- routes: int32 [4096, 2], P('ep'), may hold values from 0 to 31, as said below
- group_logits: float32 [4096, 4], P('ep'), may hold values from -6 to 6
- choice_logits: float32 [4096, 2], P('ep'), may hold values from -6 to 6
- w_gate: bfloat16 [32, 2048, 2048], P('ep', None, 'tp'), may hold values from -0.125 to 0.125
- w_up: bfloat16 [32, 2048, 2048], P('ep', None, 'tp'), may hold values from -0.125 to 0.125
- w_down: bfloat16 [32, 2048, 2048], P('ep', None, 'tp'), may hold values from -0.125 to 0.125
Outputs:
- mixer_out: bfloat16 [8192, 2048], P('ep', 'tp')
- expert_out: bfloat16 [4096, 2048], P('ep', 'tp')
Inputs may be any that keep to these rules, and one draw needn't show every extreme that they name: `routes`: in each aligned block of 128 rows (the rows of one index of ep) no expert is named by more than 16 rows, and some expert reaches that bound in every block; the 2 experts of a row differ and lie in the same group.
All inputs are finite; a program needn't handle non-finite values.
Results may differ from a plain program's by a relative error of at most 0.01.
Values may be sent and summed in bfloat16 or wider, within the bound.
A program may use at most 64 MiB of HBM per device.

v0:
```python
import jax
import jax.numpy as jnp
from jax import lax
from jax.sharding import Mesh
from jax.sharding import PartitionSpec as P

KEYDIM = 128
VDIM = 128
GROUPS = 4
TOPK = 2
BLOCK = 64
EP = ("ep_0", "ep_1")
norm_eps = 1e-06
highest_precision = lax.Precision.HIGHEST


def filled_with(shard, identity):
    return jax.tree.map(
        lambda part, zero: jnp.zeros_like(part) + jnp.asarray(zero, part.dtype), shard, identity
    )


def collected_together(shard, axis):
    leaves = jax.tree.leaves(shard)
    sequence = sorted(range(len(leaves)), key=lambda k: -leaves[k].size)
    width = (1, *leaves[sequence[0]].shape)[-1]
    lines = [
        jnp.pad(leaves[k].reshape(-1), (0, -leaves[k].size % width)).reshape(-1, width)
        for k in sequence
    ]
    both, at, found = (lax.all_gather(jnp.concatenate(lines), axis), 0, {})
    for k, line in zip(sequence, lines):
        section = both[:, at : at + len(line)].reshape(len(both), -1)
        found[k] = section[:, : leaves[k].size].reshape(-1, *leaves[k].shape)
        at += len(line)
    numbers = iter(range(len(leaves)))
    return jax.tree.map(lambda _: found[next(numbers)], shard)


def carried_in(shard, axes, combine, identity):
    before = start = filled_with(shard, identity)
    so_far = shard
    for axis in reversed(axes):
        devices, index = (lax.axis_size(axis), lax.axis_index(axis))
        pieces = collected_together(
            jax.tree.map(
                lambda part, kind: part.astype(kind), so_far, (jnp.bfloat16, jnp.bfloat16)
            ),
            axis,
        )
        inside, so_far = (start, start)
        for k in range(devices):
            passed = k < index
            so_far = combine(
                so_far, jax.tree.map(lambda part, own: part[k].astype(own.dtype), pieces, shard)
            )
            inside = jax.tree.map(lambda new, old: jnp.where(passed, new, old), so_far, inside)
        before = combine(inside, before)
    return before


def laid_out(pieces, dim):
    dims = list(pieces.shape[1:])
    dims[dim] *= pieces.shape[0]
    return jnp.moveaxis(pieces, 0, dim).reshape(dims)


def from_everyone(shard, axis):
    copies = jnp.broadcast_to(shard, (lax.axis_size(axis), *shard.shape))
    return lax.all_to_all(copies, axis, split_axis=0, concat_axis=0, tiled=True)


def gather_directly(shard, axis, dim):
    return laid_out(from_everyone(shard, axis), dim)


def rms_scale(features, gain_vec):
    return (
        features
        * lax.rsqrt(jnp.mean(features * features, axis=-1, keepdims=True) + norm_eps)
        * gain_vec
    )


def block_terms(query_block, input_block, log_blk, value_block, carried_state):
    cumulative_log = jnp.cumsum(log_blk, axis=0)
    between_block_term = jnp.einsum(
        "zug,ugr->zur",
        query_block * jnp.exp(cumulative_log),
        carried_state,
        precision=highest_precision,
    )
    causal = jnp.tril(jnp.ones((query_block.shape[0], query_block.shape[0]), dtype=bool))[
        :, :, None, None
    ]
    differ = cumulative_log[:, None] - cumulative_log[None, :]
    decays = jnp.exp(jnp.where(causal, differ, -jnp.inf))
    scores = jnp.sum(query_block[:, None] * input_block[None, :] * decays, axis=-1)
    result = between_block_term + jnp.einsum(
        "tsh,shv->thv", scores, value_block, precision=highest_precision
    )
    ending_log_decay = cumulative_log[-1]
    updated_state = jnp.exp(ending_log_decay)[..., None] * carried_state + jnp.einsum(
        "twa,twr->war",
        input_block * jnp.exp(ending_log_decay[None] - cumulative_log),
        value_block,
        precision=highest_precision,
    )
    return (updated_state, result, cumulative_log)


def mixer_local(
    mixer_query, mixer_forget, mixer_value, mixer_gate, forget_floor, head_gain, mixer_proj
):
    length = mixer_query.shape[0]
    heads_local = mixer_query.shape[1] // KEYDIM
    blocks = length // BLOCK

    def split_blocks(source_array, last_width):
        return source_array.reshape(blocks, BLOCK, heads_local, last_width)

    queries = jax.nn.silu(mixer_query.astype(jnp.float32))
    input_rates = (1.0 - forget_floor) * jax.nn.sigmoid(-mixer_forget.astype(jnp.float32))
    log_forget = jnp.log1p(-input_rates)
    value_rows = mixer_value.astype(jnp.float32)

    def advance(carry_pair, block_inputs):
        carried_state, offset_log = carry_pair
        query_block, input_block, value_block, log_blk = block_inputs
        updated_state, result, cumulative_log = block_terms(
            query_block, input_block, log_blk, value_block, carried_state
        )
        scaled_values = query_block * jnp.exp(cumulative_log + offset_log[None])
        return ((updated_state, offset_log + cumulative_log[-1]), (result, scaled_values))

    initial = (
        jnp.zeros((heads_local, KEYDIM, VDIM), jnp.float32),
        jnp.zeros((heads_local, KEYDIM), jnp.float32),
    )
    (local_state, total_log), (output_rows, scaled_values) = lax.scan(
        advance,
        initial,
        (
            split_blocks(queries, KEYDIM),
            split_blocks(input_rates, KEYDIM),
            split_blocks(value_rows, VDIM),
            split_blocks(log_forget, KEYDIM),
        ),
    )

    def combine(earlier, later):
        return (earlier[0] * later[0], later[0][..., None] * earlier[1] + later[1])

    identity = (jnp.ones_like(total_log), jnp.zeros_like(local_state))
    incoming_state = carried_in((jnp.exp(total_log), local_state), EP, combine, identity)
    output_rows = output_rows + jnp.einsum(
        "qsfa,fap->qsfp", scaled_values, incoming_state[1], precision=highest_precision
    )
    output_rows = output_rows.reshape(length, heads_local, VDIM)
    gate_act = jax.nn.silu(mixer_gate.astype(jnp.float32)).reshape(length, heads_local, VDIM)
    gated_out = rms_scale(output_rows, head_gain) * gate_act
    mixed_heads = gated_out.reshape(length, heads_local * VDIM).astype(jnp.bfloat16)
    summed = jnp.dot(
        lax.all_gather(mixed_heads, "tp", axis=1, tiled=True),
        mixer_proj,
        preferred_element_type=jnp.float32,
    )
    return summed.astype(jnp.bfloat16)


def gate_weights(routes, group_logits, choice_logits, group_size):
    group_exp = jnp.exp(group_logits)
    group_prob = group_exp / jnp.sum(group_exp, axis=-1, keepdims=True)
    groups_of = routes // group_size
    member = (groups_of[..., None] == jnp.arange(GROUPS, dtype=jnp.int32)).astype(jnp.float32)
    picked_prob = jnp.sum(member * group_prob[:, None, :], axis=-1)
    choice_exp = jnp.exp(choice_logits)
    together = (groups_of[:, :, None] == groups_of[:, None, :]).astype(jnp.float32)
    within = jnp.sum(together * choice_exp[:, None, :], axis=-1)
    return picked_prob * choice_exp / within


def finish(gate_pre, up_pre, down_local, sources, slot_count):
    hidden = (jax.nn.silu(gate_pre) * up_pre).astype(jnp.bfloat16)
    summed = jnp.dot(
        gather_directly(hidden, "tp", 1), down_local, preferred_element_type=jnp.float32
    )
    shaped = summed.astype(jnp.bfloat16).reshape(sources, slot_count, down_local.shape[1])
    return lax.all_to_all(shaped, EP, split_axis=0, concat_axis=0, tiled=True)


def expert_local(
    expert_tokens, expert_gain, routes, group_logits, choice_logits, w_gate, w_up, w_down
):
    count_rows, model_width = expert_tokens.shape
    experts_all = lax.axis_size(EP)
    capacity = 2 * TOPK * count_rows // experts_all
    normed = rms_scale(expert_tokens.astype(jnp.float32), expert_gain).astype(jnp.bfloat16)
    weights = gate_weights(routes, group_logits, choice_logits, experts_all // GROUPS)
    flat_routes = routes.reshape(-1)
    onehot = (flat_routes[:, None] == jnp.arange(experts_all, dtype=jnp.int32)).astype(jnp.int32)
    earlier = jnp.cumsum(onehot, axis=0) - onehot
    ranks = jnp.sum(earlier * onehot, axis=-1)
    slot_of = flat_routes * capacity + ranks
    token_ids = jnp.arange(flat_routes.shape[0], dtype=jnp.int32) // TOPK
    token_of = jnp.full((experts_all * capacity,), count_rows, jnp.int32).at[slot_of].set(token_ids)
    padded = jnp.concatenate([normed, jnp.zeros((1, model_width), jnp.bfloat16)], axis=0)
    outgoing = padded[token_of].reshape(experts_all, capacity, model_width)
    gate_local = w_gate[0]
    up_local = w_up[0]
    down_local = w_down[0]
    arrived = lax.all_to_all(outgoing, EP, split_axis=0, concat_axis=0, tiled=True)
    sources, slot_count, _ = arrived.shape
    flat_in = arrived.reshape(sources * slot_count, model_width)
    gate_pre = jnp.dot(flat_in, gate_local, preferred_element_type=jnp.float32)
    up_pre = jnp.dot(flat_in, up_local, preferred_element_type=jnp.float32)
    came_back = finish(gate_pre, up_pre, down_local, sources, slot_count)
    picked = (
        came_back.reshape(-1, came_back.shape[-1])[slot_of].astype(jnp.float32)
        * weights.reshape(-1)[:, None]
    )
    return jnp.sum(picked.reshape(count_rows, TOPK, -1), axis=1).astype(jnp.bfloat16)


def per_device(
    mixer_query,
    mixer_forget,
    mixer_value,
    mixer_gate,
    forget_floor,
    head_gain,
    mixer_proj,
    expert_tokens,
    expert_gain,
    routes,
    group_logits,
    choice_logits,
    w_gate,
    w_up,
    w_down,
):
    mixer_out = mixer_local(
        mixer_query, mixer_forget, mixer_value, mixer_gate, forget_floor, head_gain, mixer_proj
    )
    expert_out = expert_local(
        expert_tokens, expert_gain, routes, group_logits, choice_logits, w_gate, w_up, w_down
    )
    return (mixer_out, expert_out)


def solution(mesh):
    finer = Mesh(mesh.devices.reshape(8, 4, mesh.shape["tp"]), ("ep_0", "ep_1", "tp"))
    placed = (
        P(EP, "tp"),
        P(EP, "tp"),
        P(EP, "tp"),
        P(EP, "tp"),
        P("tp"),
        P(),
        P(None, "tp"),
        P(EP, None),
        P(),
        P(EP, None),
        P(EP, None),
        P(EP, None),
        P(EP, None, "tp"),
        P(EP, None, "tp"),
        P(EP, None, "tp"),
    )
    return jax.shard_map(
        per_device,
        mesh=finer,
        in_specs=placed,
        out_specs=(P(EP, "tp"), P(EP, "tp")),
        check_vma=False,
    )
```

profile of v0, /device:TPU:1, one launch (start us, length us, event | category | flops | bytes accessed | tf_op | source)
XLA Modules:
  0.0 173.8 jit_solution(17011988294751444505)
XLA Ops:
  7.2 0.8 copy.50
  8.3 0.7 and_select_fusion
  10.2 1.4 scatter_custom_fusion
  11.6 1.2 fusion.24
  12.9 1.2 fusion.26
  14.2 3.3 %gather_fusion = bf16[512,2048]{1,0:T(8,128)(2,1)} fusion(bf16[129,2048]{1,0:T(8,128)(2,1)S(1)} %concatenate.11, s32[1024]{0:T(1024)S(1)} %pad_clamp_fusion.1), kind=kCustom, calls=%fused_computation | custom fusion | bytes 4196352 | tf_op jit(solution)/shard_map/gather | solution.py:208
  17.5 13.8 %all-to-all-start = ((bf16[32,16,2048]{2,1,0:T(8,128)(2,1)}), bf16[32,16,2048]{2,1,0:T(8,128)(2,1)S(1)}, u32[]{:S(2)}, u32[]{:S(2)}) async-start(bf16[32,16,2048]{2,1,0:T(8,128)(2,1)} %bitcast.31), calls=%async_computation | async-start | bytes 4194304 | tf_op jit(solution)/shard_map/all_to_all | solution.py:212
  31.6 13.7 %while.17 = (s32[]{:T(128)}, f32[1,128,128]{2,1,0:T(8,128)S(1)}, f32[1,128]{1,0:T(1,128)S(1)}, f32[4,64,1,128]{3,1,2,0:T(8,128)}, f32[4,64,1,128]{3,1,2,0:T(8,12...) while((s32[]{:T(128)}, f32[1,128,128]{2,1,0:T(8,128)S(1)}, ...), condition=%wide.region_3.4_spmd.clone, body=%wide.region_0.3_spmd.clone.sunk | while | flops 34709760 | bytes 1030797 | solution.py:140
  32.4 1.4 multiply_reduce_fusion.3
  34.0 0.8 fusion.173
  35.8 1.4 multiply_reduce_fusion.3
  37.4 0.8 fusion.173
  39.2 1.4 multiply_reduce_fusion.3
  40.8 0.8 fusion.173
  42.7 1.4 multiply_reduce_fusion.3
  44.2 0.8 fusion.173
  45.4 10.6 %all-gather.2 = bf16[4,129,128]{2,1,0:T(8,128)(2,1)S(1)} all-gather(bf16[1,129,128]{2,1,0:T(8,128)(2,1)S(1)} %maximum_bitcast_fusion), channel_id=2, replica_groups=mesh['ep_0'=8,'ep_1'=4,'tp'=16] {'ep_1'}, dimensions={0}, use_global_device_ids=true | all-gather | bytes 165120 | tf_op jit(solution)/shard_map/all_gather | solution.py:31
  56.0 23.8 %all-to-all-done = bf16[32,16,2048]{2,1,0:T(8,128)(2,1)S(1)} async-done(((bf16[32,16,2048]{2,1,0:T(8,128)(2,1)}), bf16[32,16,2048]{2,1,0:T(8,128)(2,1)S(1)}, u32[]{:S(2)}, u32[]{:S(2)}) %all-to-all-start) | async-done | bytes 2097184 | tf_op jit(solution)/shard_map/all_to_all | solution.py:212
  79.9 0.7 fusion.29
  80.6 0.7 fusion.22
  81.4 1.6 broadcast_in_dim.37
  83.0 9.9 %all-to-all-start.1 = ((bf16[16,512,128]{1,2,0:T(8,128)(2,1)}), bf16[16,512,128]{1,2,0:T(8,128)(2,1)S(1)}, u32[]{:S(2)}, u32[]{:S(2)}) async-start(bf16[16,512,128]{1,2,0:T(8,128)(2,1)} %broadcast_in_dim.37), calls=%async_computation.1 | async-start | bytes 4194304 | tf_op jit(solution)/shard_map/all_to_all | solution.py:70
  93.1 20.6 %all-gather.3 = bf16[8,129,128]{2,1,0:T(8,128)(2,1)S(1)} all-gather(bf16[1,129,128]{2,1,0:T(8,128)(2,1)S(1)} %maximum_bitcast_fusion.1), channel_id=3, replica_groups=mesh['ep_0'=8,'ep_1'=4,'tp'=16] {'ep_0'}, dimensions={0}, use_global_device_ids=true | all-gather | bytes 297216 | tf_op jit(solution)/shard_map/all_gather | solution.py:31
  113.8 1.7 multiply_reduce_fusion.1
  115.6 0.7 fusion.41
  116.6 26.2 %all-to-all-done.1 = bf16[16,512,128]{1,2,0:T(8,128)(2,1)S(1)} async-done(((bf16[16,512,128]{1,2,0:T(8,128)(2,1)}), bf16[16,512,128]{1,2,0:T(8,128)(2,1)S(1)}, u32[]{:S(2)}, u32[]{:S(2)}) %all-to-all-start.1) | async-done | bytes 2097184 | tf_op jit(solution)/shard_map/all_to_all | solution.py:70
  142.8 2.4 %convolution_convert_fusion = bf16[512,128]{1,0:T(8,128)(2,1)} fusion(bf16[512,2048]{0,1:T(8,128)(2,1)S(1)} %bitcast.225, bf16[1,2048,128]{2,1,0:T(8,128)(2,1)} %param.31), kind=kOutput, calls=%fused_computation.42 | convolution fusion | flops 268500992 | bytes 2752512 | tf_op jit(solution)/shard_map/dot_general | solution.py:185
  145.2 5.1 %all-to-all-start.2 = ((bf16[32,16,128]{2,1,0:T(8,128)(2,1)}), bf16[32,16,128]{2,1,0:T(8,128)(2,1)S(1)}, u32[]{:S(2)}, u32[]{:S(2)}) async-start(bf16[32,16,128]{2,1,0:T(8,128)(2,1)} %bitcast.38), calls=%async_computation.2 | async-start | bytes 262144 | tf_op jit(solution)/shard_map/all_to_all | solution.py:189
  150.3 12.6 %all-gather.6.cloned.1.call-done = bf16[256,2048]{1,0:T(8,128)(2,1)} async-done(((bf16[256,128]{1,0:T(8,128)(2,1)}), bf16[256,2048]{1,0:T(8,128)(2,1)}) %all-gather.6.cloned.1.call-update) | async-done | bytes 1048592 | tf_op jit(solution)/shard_map/all_gather | solution.py:164
  162.9 2.3 %convolution_convert_fusion.1 = bf16[256,128]{1,0:T(8,128)(2,1)} fusion(bf16[256,2048]{1,0:T(8,128)(2,1)} %all-gather.6.cloned.1.call-done, bf16[2048,128]{1,0:T(8,128)(2,1)S(1)} %copy-done.1), kind=kOutput, calls=%fused_computation.45 | convolution fusion | flops 134250496 | bytes 1638400 | tf_op jit(solution)/shard_map/dot_general | solution.py:163
  165.2 0.9 gather_fusion.1
  166.1 0.9 fusion.38
  (114 shorter events, 7.3 us)
Async XLA Ops:
  7.2 72.7 %copy-start = (bf16[1,2048,128]{2,1,0:T(8,128)(2,1)S(1)}, bf16[1,2048,128]{2,1,0:T(8,128)(2,1)}, u32[]{:S(2)}) copy-start(bf16[1,2048,128]{2,1,0:T(8,128)(2,1)} %param.29) | copy-start | bytes 1572868
  17.5 13.9 %copy-start.10 = (f32[128]{0:T(128)S(1)}, f32[128]{0:T(128)}, u32[]{:S(2)}) copy-start(f32[128]{0:T(128)} %param.21) | copy-start | bytes 1540
  17.5 13.9 %copy-start.2 = (bf16[256,128]{1,0:T(8,128)(2,1)S(1)}, bf16[256,128]{1,0:T(8,128)(2,1)}, u32[]{:S(2)}) copy-start(bf16[256,128]{1,0:T(8,128)(2,1)} %param.19) | copy-start | bytes 196612
  17.5 14.0 %copy-start.3 = (bf16[256,128]{1,0:T(8,128)(2,1)S(1)}, bf16[256,128]{1,0:T(8,128)(2,1)}, u32[]{:S(2)}) copy-start(bf16[256,128]{1,0:T(8,128)(2,1)} %param.17) | copy-start | bytes 196612
  17.5 14.0 %copy-start.4 = (bf16[256,128]{1,0:T(8,128)(2,1)S(1)}, bf16[256,128]{1,0:T(8,128)(2,1)}, u32[]{:S(2)}) copy-start(bf16[256,128]{1,0:T(8,128)(2,1)} %param.18) | copy-start | bytes 196612
  17.5 62.3 %all-to-all-start = ((bf16[32,16,2048]{2,1,0:T(8,128)(2,1)}), bf16[32,16,2048]{2,1,0:T(8,128)(2,1)S(1)}, u32[]{:S(2)}, u32[]{:S(2)}) async-start(bf16[32,16,2048]{2,1,0:T(8,128)(2,1)} %bitcast.31), calls=%async_computation | async-start | bytes 4194304 | tf_op jit(solution)/shard_map/all_to_all | solution.py:212
  45.4 35.2 %copy-start.9 = (bf16[1,2048,128]{2,1,0:T(8,128)(2,1)S(1)}, bf16[1,2048,128]{2,1,0:T(8,128)(2,1)}, u32[]{:S(2)}) copy-start(bf16[1,2048,128]{2,1,0:T(8,128)(2,1)} %param.30) | copy-start | bytes 1572868
  83.0 32.6 %copy-start.5 = (bf16[256,128]{1,0:T(8,128)(2,1)S(1)}, bf16[256,128]{1,0:T(8,128)(2,1)}, u32[]{:S(2)}) copy-start(bf16[256,128]{1,0:T(8,128)(2,1)} %param.20) | copy-start | bytes 196612
  83.0 32.6 %copy-start.8 = (f32[128]{0:T(128)S(1)}, f32[128]{0:T(128)}, u32[]{:S(2)}) copy-start(f32[128]{0:T(128)} %param.22) | copy-start | bytes 1540
  83.0 59.8 %all-to-all-start.1 = ((bf16[16,512,128]{1,2,0:T(8,128)(2,1)}), bf16[16,512,128]{1,2,0:T(8,128)(2,1)S(1)}, u32[]{:S(2)}, u32[]{:S(2)}) async-start(bf16[16,512,128]{1,2,0:T(8,128)(2,1)} %broadcast_in_dim.37), calls=%async_computation.1 | async-start | bytes 4194304 | tf_op jit(solution)/shard_map/all_to_all | solution.py:70
  92.9 23.5 %copy-start.7 = (f32[128,2]{0,1:T(2,128)S(1)}, f32[128,2]{0,1:T(2,128)}, u32[]{:S(2)}) copy-start(f32[128,2]{0,1:T(2,128)} %param.28) | copy-start | bytes 3076
  92.9 23.5 %copy-start.6 = (f32[128,4]{0,1:T(4,128)S(1)}, f32[128,4]{0,1:T(4,128)}, u32[]{:S(2)}) copy-start(f32[128,4]{0,1:T(4,128)} %param.27) | copy-start | bytes 6148
  92.9 70.0 %all-gather.6.cloned.1.call-start = ((), (), s32[]{:S(2)}) async-start(), calls=%async_computation.3 | async-start | bytes 1114112 | tf_op jit(solution)/shard_map/all_gather | solution.py:164
  113.8 49.2 %copy-start.1 = (bf16[2048,128]{1,0:T(8,128)(2,1)S(1)}, bf16[2048,128]{1,0:T(8,128)(2,1)}, u32[]{:S(2)}) copy-start(bf16[2048,128]{1,0:T(8,128)(2,1)} %param.23) | copy-start | bytes 1572868
  145.2 20.0 %all-to-all-start.2 = ((bf16[32,16,128]{2,1,0:T(8,128)(2,1)}), bf16[32,16,128]{2,1,0:T(8,128)(2,1)S(1)}, u32[]{:S(2)}, u32[]{:S(2)}) async-start(bf16[32,16,128]{2,1,0:T(8,128)(2,1)} %bitcast.38), calls=%async_computation.2 | async-start | bytes 262144 | tf_op jit(solution)/shard_map/all_to_all | solution.py:189
Sparse Core Ops, SparseCore 0:
  116.4 46.4 all-gather.5
where the time goes:
time: 174 us
  waiting for transfers between devices  62.6 us (36%)
  blocking collectives  31.2 us (18%)
  starting transfers between devices  28.9 us (17%)
  between operations  14.4 us (8%)
  other arithmetic  14.2 us (8%)
  matrix products  12.9 us (7%)
  local copies, waits for them, and re-layouts  9.24 us (5%)
    all_gather x2, blocking collectives, collected_together(): both, at, found = (lax.all_gather(jnp.concatenate(lines), axis), 0, {})  31.2 us
    all_to_all x1, waiting for transfers between devices, from_everyone(): return lax.all_to_all(copies, axis, split_axis=0, concat_axis=0, tiled=True)  26.2 us
    all_to_all x1, waiting for transfers between devices, expert_local(): lax.all_to_all(outgoing, EP, split_axis=0, concat_axis=0, tiled=True)  23.8 us
    all_to_all x1, starting transfers between devices, expert_local(): lax.all_to_all(outgoing, EP, split_axis=0, concat_axis=0, tiled=True)  13.8 us
    all_gather x1, waiting for transfers between devices, mixer_local(): lax.all_gather(mixed_heads, 'tp', axis=1, tiled=True)  12.6 us
    all_to_all x1, starting transfers between devices, from_everyone(): return lax.all_to_all(copies, axis, split_axis=0, concat_axis=0, tiled=True)  9.89 us
    reduce_sum x4, other arithmetic, block_terms(): jnp.sum(query_block[:, None] * input_block[None, :] * decays, axis=-1)  5.4 us
    all_to_all x1, starting transfers between devices, finish(): return lax.all_to_all(shaped, EP, split_axis=0, concat_axis=0, tiled=True)  5.08 us
  transfers between devices with their start and end apart: 4, of which 3 were waited for; matrix products, arithmetic and copies ran while one was open for 12% of the time, Pallas kernels for 0%

commit v1 on v0

--- a/solution.py
+++ b/solution.py
@@ -12,6 +12,7 @@
 EP = ("ep_0", "ep_1")
 norm_eps = 1e-06
 highest_precision = lax.Precision.HIGHEST
+lead_marks_on = lambda inp, array_dim: jnp.concatenate(lax.all_gather(inp, "tp"), axis=array_dim)
 
 
 def filled_with(shard, identity):
@@ -160,11 +161,7 @@
     gate_act = jax.nn.silu(mixer_gate.astype(jnp.float32)).reshape(length, heads_local, VDIM)
     gated_out = rms_scale(output_rows, head_gain) * gate_act
     mixed_heads = gated_out.reshape(length, heads_local * VDIM).astype(jnp.bfloat16)
-    summed = jnp.dot(
-        lax.all_gather(mixed_heads, "tp", axis=1, tiled=True),
-        mixer_proj,
-        preferred_element_type=jnp.float32,
-    )
+    summed = jnp.dot(lead_marks_on(mixed_heads, 1), mixer_proj, preferred_element_type=jnp.float32)
     return summed.astype(jnp.bfloat16)
 
 

time: 174 us -> 193 us (1.11)
  waiting for transfers between devices: 62.6 us -> 78.4 us
  matrix products: 12.9 us -> 9.47 us
  blocking collectives: 31.2 us -> 34.6 us
  local copies, waits for them, and re-layouts: 9.24 us -> 11.9 us
  starting transfers between devices: 28.9 us -> 31.5 us
  other arithmetic: 14.2 us -> 11.7 us
    all_gather x1, waiting for transfers between devices: 12.6 us -> 46.1 us  [lax.all_gather(inp, 'tp')]
    all_to_all x1, waiting for transfers between devices: 26.2 us -> 0.01 us  [from_everyone(): return lax.all_to_all(copies, axis, split_axis=0, concat_axis=0, tiled=True)]
    all_to_all x1, waiting for transfers between devices: 0.01 us -> 7.1 us  [finish(): return lax.all_to_all(shaped, EP, split_axis=0, concat_axis=0, tiled=True)]
    all_gather x2, blocking collectives: 31.2 us -> 34.6 us  [collected_together(): both, at, found = (lax.all_gather(jnp.concatenate(lines), axis), 0, {})]
    all_to_all x1, starting transfers between devices: 5.08 us -> 7.7 us  [finish(): return lax.all_to_all(shaped, EP, split_axis=0, concat_axis=0, tiled=True)]
    dot_general x4, matrix products: 3.09 us -> 0.67 us  [block_terms(): jnp.einsum('tsh,shv->thv', scores, value_block, precision=highest_precision)]
    dynamic_update_slice x4, other arithmetic: 2.49 us -> 0.08 us  [mixer_local(): lax.scan(advance, initial, (split_blocks(queries, KEYDIM), split_blocks(i...]
    reshape x0 -> x1, local copies, waits for them, and re-layouts: none -> 2.34 us  [jnp.concatenate(lax.all_gather(inp, 'tp'), axis=array_dim)]
  transfers between devices with their start and end apart: 4 -> 4, of which waited for: 3 -> 3; matrix products, arithmetic and copies ran while one was open for 12% -> 8% of each run, Pallas kernels for 0% -> 0%
where the time goes in v1:
time: 193 us; the launch traced here: 192 us
  waiting for transfers between devices  78.4 us (41%)
  blocking collectives  34.6 us (18%)
  starting transfers between devices  31.5 us (16%)
  between operations  14.4 us (7%)
  local copies, waits for them, and re-layouts  11.9 us (6%)
  other arithmetic  11.7 us (6%)
  matrix products  9.47 us (5%)
    all_gather x1, waiting for transfers between devices, lax.all_gather(inp, 'tp')  46.1 us
    all_gather x2, blocking collectives, collected_together(): both, at, found = (lax.all_gather(jnp.concatenate(lines), axis), 0, {})  34.6 us
    all_to_all x1, waiting for transfers between devices, expert_local(): lax.all_to_all(outgoing, EP, split_axis=0, concat_axis=0, tiled=True)  25.2 us
    all_to_all x1, starting transfers between devices, expert_local(): lax.all_to_all(outgoing, EP, split_axis=0, concat_axis=0, tiled=True)  13.8 us
    all_to_all x1, starting transfers between devices, from_everyone(): return lax.all_to_all(copies, axis, split_axis=0, concat_axis=0, tiled=True)  9.89 us
    all_to_all x1, starting transfers between devices, finish(): return lax.all_to_all(shaped, EP, split_axis=0, concat_axis=0, tiled=True)  7.7 us
    all_to_all x1, waiting for transfers between devices, finish(): return lax.all_to_all(shaped, EP, split_axis=0, concat_axis=0, tiled=True)  7.1 us
    reduce_sum x4, other arithmetic, block_terms(): jnp.sum(query_block[:, None] * input_block[None, :] * decays, axis=-1)  5.33 us
  transfers between devices with their start and end apart: 4, of which 3 were waited for; matrix products, arithmetic and copies ran while one was open for 8% of the time, Pallas kernels for 0%

profile of v1, /device:TPU:1, one launch (start us, length us, event | category | flops | bytes accessed | tf_op | source)
XLA Modules:
  0.0 192.4 jit_solution(7422716623838126194)
XLA Ops:
  7.2 0.8 copy.74
  8.3 0.7 and_select_fusion
  9.0 0.6 reduce-window.6
  10.2 1.4 scatter_custom_fusion
  11.6 1.2 fusion.24
  12.9 1.2 fusion.26
  14.2 3.3 %gather_fusion = bf16[512,2048]{1,0:T(8,128)(2,1)} fusion(bf16[129,2048]{1,0:T(8,128)(2,1)S(1)} %concatenate.11, s32[1024]{0:T(1024)S(1)} %pad_clamp_fusion.1), kind=kCustom, calls=%fused_computation | custom fusion | bytes 4196352 | tf_op jit(solution)/shard_map/gather | solution.py:205
  17.5 13.8 %all-to-all-start = ((bf16[32,16,2048]{2,1,0:T(8,128)(2,1)}), bf16[32,16,2048]{2,1,0:T(8,128)(2,1)S(1)}, u32[]{:S(2)}, u32[]{:S(2)}) async-start(bf16[32,16,2048]{2,1,0:T(8,128)(2,1)} %bitcast.37), calls=%async_computation | async-start | bytes 4194304 | tf_op jit(solution)/shard_map/all_to_all | solution.py:209
  31.6 9.0 %while.17 = (s32[]{:T(128)}, f32[1,128,128]{2,1,0:T(8,128)S(1)}, f32[1,128]{1,0:T(1,128)S(1)}, f32[4,64,1,128]{3,1,2,0:T(8,128)S(1)}, f32[4,64,1,128]{3,1,2,0:T(...) while((s32[]{:T(128)}, f32[1,128,128]{2,1,0:T(8,128)S(1)}, ...), condition=%wide.region_3.4_spmd.clone, body=%wide.region_0.3_spmd.clone.sunk | while | flops 34709760 | bytes 1046165 | solution.py:141
  31.8 1.3 multiply_reduce_fusion.3
  33.6 0.3 fusion.171
  34.1 1.3 multiply_reduce_fusion.3
  36.3 1.3 multiply_reduce_fusion.3
  38.5 1.3 multiply_reduce_fusion.3
  40.7 14.0 %all-gather.3 = bf16[4,129,128]{2,1,0:T(8,128)(2,1)S(1)} all-gather(bf16[1,129,128]{2,1,0:T(8,128)(2,1)S(1)} %maximum_bitcast_fusion), channel_id=2, replica_groups=mesh['ep_0'=8,'ep_1'=4,'tp'=16] {'ep_1'}, dimensions={0}, use_global_device_ids=true | all-gather | bytes 165120 | tf_op jit(solution)/shard_map/all_gather | solution.py:32
  54.7 25.2 %all-to-all-done = bf16[32,16,2048]{2,1,0:T(8,128)(2,1)S(1)} async-done(((bf16[32,16,2048]{2,1,0:T(8,128)(2,1)}), bf16[32,16,2048]{2,1,0:T(8,128)(2,1)S(1)}, u32[]{:S(2)}, u32[]{:S(2)}) %all-to-all-start) | async-done | bytes 2097184 | tf_op jit(solution)/shard_map/all_to_all | solution.py:209
  79.9 0.7 fusion.29
  80.6 0.3 copy-done.9
  80.9 0.7 fusion.22
  81.7 1.6 broadcast_in_dim.37
  83.3 9.9 %all-to-all-start.1 = ((bf16[16,512,128]{1,2,0:T(8,128)(2,1)}), bf16[16,512,128]{1,2,0:T(8,128)(2,1)S(1)}, u32[]{:S(2)}, u32[]{:S(2)}) async-start(bf16[16,512,128]{1,2,0:T(8,128)(2,1)} %broadcast_in_dim.37), calls=%async_computation.1 | async-start | bytes 4194304 | tf_op jit(solution)/shard_map/all_to_all | solution.py:71
  93.4 20.6 %all-gather.4 = bf16[8,129,128]{2,1,0:T(8,128)(2,1)S(1)} all-gather(bf16[1,129,128]{2,1,0:T(8,128)(2,1)S(1)} %maximum_bitcast_fusion.1), channel_id=3, replica_groups=mesh['ep_0'=8,'ep_1'=4,'tp'=16] {'ep_0'}, dimensions={0}, use_global_device_ids=true | all-gather | bytes 297216 | tf_op jit(solution)/shard_map/all_gather | solution.py:32
  114.0 0.7 multiply_reduce_fusion.1
  114.8 0.7 fusion.41
  115.8 46.1 %all-gather.7.cloned.1.call-done = bf16[4096,128]{1,0:T(8,128)(2,1)} async-done(((bf16[256,128]{1,0:T(8,128)(2,1)}), bf16[4096,128]{1,0:T(8,128)(2,1)}) %all-gather.7.cloned.1.call-update) | async-done | bytes 1048592 | tf_op jit(solution)/shard_map/all_gather | solution.py:15
  161.9 2.3 %copy.72 = bf16[256,16,128]{0,2,1:T(8,128)(2,1)} copy(bf16[256,16,128]{2,0,1:T(8,128)(2,1)} %bitcast.243) | data formatting | bytes 2097152 | tf_op jit(solution)/shard_map/reshape | solution.py:15
  164.2 2.4 %convolution_convert_fusion = bf16[512,128]{1,0:T(8,128)(2,1)} fusion(bf16[512,2048]{0,1:T(8,128)(2,1)S(1)} %bitcast.235, bf16[1,2048,128]{2,1,0:T(8,128)(2,1)} %param.31), kind=kOutput, calls=%fused_computation.42 | convolution fusion | flops 268500992 | bytes 2752512 | tf_op jit(solution)/shard_map/dot_general | solution.py:182
  166.7 7.7 %all-to-all-start.2 = ((bf16[32,16,128]{2,1,0:T(8,128)(2,1)}), bf16[32,16,128]{2,1,0:T(8,128)(2,1)S(1)}, u32[]{:S(2)}, u32[]{:S(2)}) async-start(bf16[32,16,128]{2,1,0:T(8,128)(2,1)} %bitcast.44), calls=%async_computation.2 | async-start | bytes 262144 | tf_op jit(solution)/shard_map/all_to_all | solution.py:186
  174.4 2.3 %convolution_convert_fusion.1 = bf16[256,128]{1,0:T(8,128)(2,1)} fusion(bf16[256,2048]{0,1:T(8,128)(2,1)} %bitcast.238, bf16[2048,128]{1,0:T(8,128)(2,1)S(1)} %copy-done.1), kind=kOutput, calls=%fused_computation.45 | convolution fusion | flops 134250496 | bytes 1638400 | tf_op jit(solution)/shard_map/dot_general | solution.py:164
  176.7 7.1 %all-to-all-done.2 = bf16[32,16,128]{2,1,0:T(8,128)(2,1)S(1)} async-done(((bf16[32,16,128]{2,1,0:T(8,128)(2,1)}), bf16[32,16,128]{2,1,0:T(8,128)(2,1)S(1)}, u32[]{:S(2)}, u32[]{:S(2)}) %all-to-all-start.2) | async-done | bytes 131104 | tf_op jit(solution)/shard_map/all_to_all | solution.py:186
  183.8 0.9 gather_fusion.1
  184.7 0.9 fusion.38
  (115 shorter events, 4.7 us)
Async XLA Ops:
  7.2 72.7 %copy-start = (bf16[1,2048,128]{2,1,0:T(8,128)(2,1)S(1)}, bf16[1,2048,128]{2,1,0:T(8,128)(2,1)}, u32[]{:S(2)}) copy-start(bf16[1,2048,128]{2,1,0:T(8,128)(2,1)} %param.29) | copy-start | bytes 1572868
  17.5 13.9 %copy-start.10 = (f32[128]{0:T(128)S(1)}, f32[128]{0:T(128)}, u32[]{:S(2)}) copy-start(f32[128]{0:T(128)} %param.21) | copy-start | bytes 1540
  17.5 13.9 %copy-start.2 = (bf16[256,128]{1,0:T(8,128)(2,1)S(1)}, bf16[256,128]{1,0:T(8,128)(2,1)}, u32[]{:S(2)}) copy-start(bf16[256,128]{1,0:T(8,128)(2,1)} %param.19) | copy-start | bytes 196612
  17.5 14.0 %copy-start.3 = (bf16[256,128]{1,0:T(8,128)(2,1)S(1)}, bf16[256,128]{1,0:T(8,128)(2,1)}, u32[]{:S(2)}) copy-start(bf16[256,128]{1,0:T(8,128)(2,1)} %param.17) | copy-start | bytes 196612
  17.5 14.0 %copy-start.4 = (bf16[256,128]{1,0:T(8,128)(2,1)S(1)}, bf16[256,128]{1,0:T(8,128)(2,1)}, u32[]{:S(2)}) copy-start(bf16[256,128]{1,0:T(8,128)(2,1)} %param.18) | copy-start | bytes 196612
  17.5 62.3 %all-to-all-start = ((bf16[32,16,2048]{2,1,0:T(8,128)(2,1)}), bf16[32,16,2048]{2,1,0:T(8,128)(2,1)S(1)}, u32[]{:S(2)}, u32[]{:S(2)}) async-start(bf16[32,16,2048]{2,1,0:T(8,128)(2,1)} %bitcast.37), calls=%async_computation | async-start | bytes 4194304 | tf_op jit(solution)/shard_map/all_to_all | solution.py:209
  79.9 1.0 copy-start.9
  83.3 31.5 %copy-start.5 = (bf16[256,128]{1,0:T(8,128)(2,1)S(1)}, bf16[256,128]{1,0:T(8,128)(2,1)}, u32[]{:S(2)}) copy-start(bf16[256,128]{1,0:T(8,128)(2,1)} %param.20) | copy-start | bytes 196612
  83.3 31.5 %copy-start.8 = (f32[128]{0:T(128)S(1)}, f32[128]{0:T(128)}, u32[]{:S(2)}) copy-start(f32[128]{0:T(128)} %param.22) | copy-start | bytes 1540
  83.3 80.9 %all-to-all-start.1 = ((bf16[16,512,128]{1,2,0:T(8,128)(2,1)}), bf16[16,512,128]{1,2,0:T(8,128)(2,1)S(1)}, u32[]{:S(2)}, u32[]{:S(2)}) async-start(bf16[16,512,128]{1,2,0:T(8,128)(2,1)} %broadcast_in_dim.37), calls=%async_computation.1 | async-start | bytes 4194304 | tf_op jit(solution)/shard_map/all_to_all | solution.py:71
  93.2 22.4 %copy-start.7 = (f32[128,2]{0,1:T(2,128)S(1)}, f32[128,2]{0,1:T(2,128)}, u32[]{:S(2)}) copy-start(f32[128,2]{0,1:T(2,128)} %param.28) | copy-start | bytes 3076
  93.2 22.4 %copy-start.6 = (f32[128,4]{0,1:T(4,128)S(1)}, f32[128,4]{0,1:T(4,128)}, u32[]{:S(2)}) copy-start(f32[128,4]{0,1:T(4,128)} %param.27) | copy-start | bytes 6148
  93.2 68.7 %all-gather.7.cloned.1.call-start = ((), (), s32[]{:S(2)}) async-start(), calls=%async_computation.3 | async-start | bytes 1114112 | tf_op jit(solution)/shard_map/all_gather | solution.py:15
  161.9 12.5 %copy-start.1 = (bf16[2048,128]{1,0:T(8,128)(2,1)S(1)}, bf16[2048,128]{1,0:T(8,128)(2,1)}, u32[]{:S(2)}) copy-start(bf16[2048,128]{1,0:T(8,128)(2,1)} %param.23) | copy-start | bytes 1572868
  166.7 17.2 %all-to-all-start.2 = ((bf16[32,16,128]{2,1,0:T(8,128)(2,1)}), bf16[32,16,128]{2,1,0:T(8,128)(2,1)S(1)}, u32[]{:S(2)}, u32[]{:S(2)}) async-start(bf16[32,16,128]{2,1,0:T(8,128)(2,1)} %bitcast.44), calls=%async_computation.2 | async-start | bytes 262144 | tf_op jit(solution)/shard_map/all_to_all | solution.py:186
Sparse Core Ops, SparseCore 0:
  115.7 46.1 all-gather.6
